TPU v7x, 32 devices: a whole 2x2x4 slice. The times are simulated.
32 devices in a mesh: sp: 8 (over z, y), tp: 4 (over x, core).
Axes of the slice: x: 2, y: 2, z: 4, core: 2. Of those that a mesh axis runs over, the one named last changes fastest.
Arguments:
- target: bfloat16 [56, 2048], P('sp'), may hold values from -6 to 6
- source: bfloat16 [2048, 2048], P('sp'), may hold values from -6 to 6
- tgt_gain: float32 [2, 2048], replicated, may hold values from 0.1 to 1.9
- src_gain: float32 [2, 2048], replicated, may hold values from 0.1 to 1.9
- w_query: bfloat16 [2, 2048, 2048], P(None, None, 'tp'), may hold values from -0.125 to 0.125
- w_key: bfloat16 [2, 2048, 2048], P(None, None, 'tp'), may hold values from -0.125 to 0.125
- w_value: bfloat16 [2, 2048, 2048], P(None, None, 'tp'), may hold values from -0.125 to 0.125
- w_out: bfloat16 [2, 2048, 2048], P(None, 'tp'), may hold values from -0.125 to 0.125
- score_scale: float32 [2, 8], P(None, 'tp'), may hold values from 1.5 to 4
Outputs:
- result: bfloat16 [56, 2048], P('sp')
All inputs are finite; a program needn't handle non-finite values.
Results may differ from a plain program's by a relative error of at most 0.015.
Values may be sent and summed in bfloat16 or wider, within the bound.
A program may use at most 64 MiB of HBM per device.

v0:
```python
import math
import jax
import jax.numpy as jnp
from jax import lax
from jax.sharding import PartitionSpec as P

HEAD_DIM = 256
EPS = 1e-06


def row_scale(values):
    return lax.rsqrt(jnp.mean(values * values, axis=-1, keepdims=True) + EPS)


def head_norm(projected):
    heads = projected.reshape(projected.shape[0], -1, HEAD_DIM)
    heads = heads * row_scale(heads)
    return heads.reshape(projected.shape).astype(jnp.bfloat16)


def source_side(src_float, src_scale, gain_row, key_weight, value_weight):
    normed_src = (src_float * src_scale * gain_row).astype(jnp.bfloat16)
    key_rows = head_norm(jnp.dot(normed_src, key_weight, preferred_element_type=jnp.float32))
    value_rows = jnp.dot(normed_src, value_weight, preferred_element_type=jnp.float32).astype(
        jnp.bfloat16
    )
    return (key_rows, value_rows)


def attend(queries, key_rows, value_rows, scales):
    root = math.sqrt(HEAD_DIM)
    count = queries.shape[0]
    local_heads = scales.shape[0]
    query_heads = queries.reshape(count, local_heads, HEAD_DIM)
    key_heads = key_rows.reshape(key_rows.shape[0], local_heads, HEAD_DIM)
    value_heads = value_rows.reshape(value_rows.shape[0], local_heads, HEAD_DIM)
    scores = jnp.einsum("qhd,khd->hqk", query_heads, key_heads, preferred_element_type=jnp.float32)
    logits = scales[:, None, None] * (scores / root - root)
    weights = jnp.exp(logits)
    denominators = jnp.sum(weights, axis=2).T
    numerators = jnp.einsum(
        "hqk,khd->qhd",
        weights.astype(jnp.bfloat16),
        value_heads,
        preferred_element_type=jnp.float32,
    )
    return (numerators.reshape(count, local_heads * HEAD_DIM), denominators)


def place(terms):
    numer_all = terms[0]
    denom_all = terms[1]
    return (numer_all, denom_all)


def body(target, source, tgt_gain, src_gain, w_query, w_key, w_value, w_out, score_scale):
    local_heads = w_query.shape[2] // HEAD_DIM
    width = local_heads * HEAD_DIM
    tok_rows = target.shape[0]
    layer_count = w_query.shape[0]
    src_float = source.astype(jnp.float32)
    src_scale = row_scale(src_float)
    hidden = target
    for layer_index in range(layer_count):
        key_rows, value_rows = source_side(
            src_float, src_scale, src_gain[layer_index], w_key[layer_index], w_value[layer_index]
        )
        scales = score_scale[layer_index]
        hidden_float = hidden.astype(jnp.float32)
        normed_tgt = (hidden_float * row_scale(hidden_float) * tgt_gain[layer_index]).astype(
            jnp.bfloat16
        )
        weight_now = w_query[layer_index]
        query_rows = head_norm(jnp.dot(normed_tgt, weight_now, preferred_element_type=jnp.float32))
        running = place(
            attend(
                lax.all_gather(query_rows, "sp", axis=0, tiled=True), key_rows, value_rows, scales
            )
        )
        numerators, denominators = (
            lax.psum_scatter(running[0], "sp", scatter_dimension=0, tiled=True),
            lax.psum_scatter(running[1], "sp", scatter_dimension=0, tiled=True),
        )
        attended = (
            (numerators.reshape(tok_rows, local_heads, HEAD_DIM) / denominators[:, :, None])
            .reshape(tok_rows, width)
            .astype(jnp.bfloat16)
        )
        share = jnp.dot(attended, w_out[layer_index], preferred_element_type=jnp.float32).astype(
            jnp.bfloat16
        )
        branch = lax.psum(share.astype(jnp.float32).astype(jnp.bfloat16), "tp").astype(jnp.float32)
        hidden = (hidden_float + branch).astype(jnp.bfloat16)
    return hidden


def solution(mesh):
    placed = (
        P("sp", None),
        P("sp", None),
        P(),
        P(),
        P(None, None, "tp"),
        P(None, None, "tp"),
        P(None, None, "tp"),
        P(None, "tp", None),
        P(None, "tp"),
    )
    return jax.shard_map(body, mesh=mesh, in_specs=placed, out_specs=P("sp", None), check_vma=False)
```

profile of v0, /device:TPU:0, one launch (start us, length us, event | category | flops | bytes accessed | tf_op | source)
XLA Modules:
  0.0 235.5 jit_solution(8419340724434277195)
XLA Ops:
  0.0 1.5 fusion.6
  1.5 0.8 fusion.73
  2.3 3.8 %slice_bitcast_fusion.2 = (bf16[512,2048]{0,1:T(8,128)(2,1)S(1)}, bf16[512,2048]{0,1:T(8,128)(2,1)}) fusion(bf16[2,2048,512]{2,1,0:T(8,128)(2,1)} %param.14), kind=kLoop, calls=%fused_computation.20 | loop fusion | bytes 8388608 | tf_op jit(solution)/shard_map/dot_general | solution.py:23
  6.2 2.5 %copy.31 = bf16[512,2048]{1,0:T(8,128)(2,1)} copy(bf16[512,2048]{0,1:T(8,128)(2,1)S(1)} %get-tuple-element.7) | data formatting | bytes 4194304 | tf_op jit(solution)/shard_map/dot_general | solution.py:23
  8.6 3.4 %multiply_reduce_fusion.1 = (f32[256,2]{0,1:T(2,128)S(1)}, f32[256,2,256]{0,2,1:T(8,128)}) fusion(bf16[2,256,2048]{2,1,0:T(8,128)(2,1)} %bitcast.104, f32[2048]{0:T(1024)S(1)} %bitcast.117, f32[256]{0:T(256)S(1)} %add_rsqrt_fusion.4, bf16[256,2048]{1,0:T(8,128)(2,1)S(1)} %copy-done.3), kind=kOutput, calls=%fused_computation.42 | convolution fusion | flops 539229696 | bytes 3681280 | tf_op jit(solution)/shard_map/dot_general | solution.py:23
  12.0 2.3 slice_bitcast_fusion.3
  14.3 2.9 %copy.30 = bf16[512,2048]{1,0:T(8,128)(2,1)S(1)} copy(bf16[512,2048]{0,1:T(8,128)(2,1)} %get-tuple-element.5) | data formatting | bytes 4194304 | tf_op jit(solution)/shard_map/dot_general | solution.py:74
  18.3 32.4 %all-gather = bf16[8,7,512]{2,1,0:T(8,128)(2,1)S(1)} all-gather(bf16[1,7,512]{2,1,0:T(8,128)(2,1)S(1)} %bitcast.113), channel_id=1, replica_groups=mesh['sp'=8,'tp'=4] {'sp'}, dimensions={0}, use_global_device_ids=true | all-gather | bytes 64512 | tf_op jit(solution)/shard_map/all_gather | solution.py:77
  50.7 2.5 %fusion.17 = bf16[256,512]{1,0:T(8,128)(2,1)S(1)} fusion(bf16[2,2048,512]{2,1,0:T(8,128)(2,1)} %param.15, bf16[256,2048]{1,0:T(8,128)(2,1)S(1)} %copy-done.3, f32[2048]{0:T(1024)S(1)} %bitcast.118, f32[256]{0:T(256)S(1)} %add_rsqrt_fusion.4), kind=kOutput, calls=%fused_computation.23 | convolution fusion | flops 539099136 | bytes 3417088 | tf_op jit(solution)/shard_map/dot_general | solution.py:24
  53.7 22.6 %fusion = f32[8,512]{1,0:T(8,128)S(1)} fusion(f32[56,512]{1,0:T(8,128)S(1)} %bitcast.105), kind=kCustom, calls=%all-reduce-scatter | all-reduce-scatter fusion | flops 32769 | bytes 131584
  76.3 1.3 collective-permute-start
  77.7 33.7 %all-reduce.1 = f32[56,2]{1,0:T(8,128)S(1)} all-reduce(f32[56,2]{1,0:T(8,128)S(1)} %copy.36), channel_id=3, replica_groups=mesh['sp'=8,'tp'=4] {'sp'}, use_global_device_ids=true, to_apply=%region_6.0.clone | all-reduce | flops 112 | bytes 896
  112.7 2.5 %copy.38 = bf16[512,2048]{1,0:T(8,128)(2,1)} copy(bf16[512,2048]{0,1:T(8,128)(2,1)S(1)} %copy-done) | data formatting | bytes 4194304 | tf_op jit(solution)/shard_map/dot_general | solution.py:23
  115.2 2.5 %fusion.20 = bf16[256,512]{1,0:T(8,128)(2,1)S(1)} fusion(bf16[2,2048,512]{2,1,0:T(8,128)(2,1)} %param.15, bf16[256,2048]{1,0:T(8,128)(2,1)S(1)} %copy-done.3, f32[2048]{0:T(1024)S(1)} %bitcast.115, f32[256]{0:T(256)S(1)} %add_rsqrt_fusion.4), kind=kOutput, calls=%fused_computation.24 | convolution fusion | flops 539099136 | bytes 3417088 | tf_op jit(solution)/shard_map/dot_general | solution.py:24
  117.7 1.6 multiply_reduce_fusion
  120.0 2.9 %copy.37 = bf16[512,2048]{1,0:T(8,128)(2,1)S(1)} copy(bf16[512,2048]{0,1:T(8,128)(2,1)} %get-tuple-element.6) | data formatting | bytes 4194304 | tf_op jit(solution)/shard_map/dot_general | solution.py:74
  123.1 2.0 convolution_convert_fusion.1
  125.1 10.3 %psum.14 = bf16[7,2048]{1,0:T(8,128)(2,1)S(1)} all-reduce(bf16[7,2048]{1,0:T(8,128)(2,1)S(1)} %convolution_convert_fusion.1), channel_id=1, replica_groups=mesh['sp'=8,'tp'=4] {'tp'}, use_global_device_ids=true, to_apply=%region_7.0 | all-reduce | flops 14336 | bytes 57344 | tf_op jit(solution)/shard_map/psum | solution.py:92
  136.3 30.5 %all-gather.1 = bf16[8,7,512]{2,1,0:T(8,128)(2,1)S(1)} all-gather(bf16[1,7,512]{2,1,0:T(8,128)(2,1)S(1)} %bitcast.114), channel_id=1, replica_groups=mesh['sp'=8,'tp'=4] {'sp'}, dimensions={0}, use_global_device_ids=true | all-gather | bytes 64512 | tf_op jit(solution)/shard_map/all_gather | solution.py:77
  167.4 19.9 %fusion.1 = f32[8,512]{1,0:T(8,128)S(1)} fusion(f32[56,512]{1,0:T(8,128)S(1)} %bitcast.106), kind=kCustom, calls=%all-reduce-scatter.1 | all-reduce-scatter fusion | flops 32769 | bytes 131584
  187.3 1.9 collective-permute-start.1
  189.3 33.1 %all-reduce.3 = f32[56,2]{1,0:T(8,128)S(1)} all-reduce(f32[56,2]{1,0:T(8,128)S(1)} %copy.43), channel_id=5, replica_groups=mesh['sp'=8,'tp'=4] {'sp'}, use_global_device_ids=true, to_apply=%region_13.0.clone | all-reduce | flops 112 | bytes 896
  222.6 2.0 convolution_convert_fusion
  224.6 10.3 %psum.15 = bf16[7,2048]{1,0:T(8,128)(2,1)S(1)} all-reduce(bf16[7,2048]{1,0:T(8,128)(2,1)S(1)} %convolution_convert_fusion), channel_id=1, replica_groups=mesh['sp'=8,'tp'=4] {'tp'}, use_global_device_ids=true, to_apply=%region_14.0 | all-reduce | flops 14336 | bytes 57344 | tf_op jit(solution)/shard_map/psum | solution.py:92
  (59 shorter events, 4.8 us)
Async XLA Ops:
  6.2 2.5 %copy-start.3 = (bf16[256,2048]{1,0:T(8,128)(2,1)S(1)}, bf16[256,2048]{1,0:T(8,128)(2,1)}, u32[]{:S(2)}) copy-start(bf16[256,2048]{1,0:T(8,128)(2,1)} %param.10) | copy-start | bytes 3145732
  8.6 3.4 %copy-start.1 = (bf16[2,2048,512]{2,1,0:T(8,128)(2,1)S(1)}, bf16[2,2048,512]{2,1,0:T(8,128)(2,1)}, u32[]{:S(2)}) copy-start(bf16[2,2048,512]{2,1,0:T(8,128)(2,1)} %param.13) | copy-start | bytes 12582916
  14.3 3.0 %copy-start.7 = (f32[2,2048]{1,0:T(2,128)S(1)}, f32[2,2048]{1,0:T(2,128)}, u32[]{:S(2)}) copy-start(f32[2,2048]{1,0:T(2,128)} %param.11) | copy-start | bytes 49156
  14.3 3.0 %copy-start.4 = (bf16[7,2048]{1,0:T(8,128)(2,1)S(1)}, bf16[7,2048]{1,0:T(8,128)(2,1)}, u32[]{:S(2)}) copy-start(bf16[7,2048]{1,0:T(8,128)(2,1)} %param.9) | copy-start | bytes 86020
  17.3 33.4 %copy-start.9 = (f32[2,2]{1,0:T(2,128)S(1)}, f32[2,2]{1,0:T(2,128)}, u32[]{:S(2)}) copy-start(f32[2,2]{1,0:T(2,128)} %param.17) | copy-start | bytes 52
  50.7 2.5 %copy-start.6 = (f32[256,2,256]{0,2,1:T(8,128)S(1)}, f32[256,2,256]{0,2,1:T(8,128)}, u32[]{:S(2)}) copy-start(f32[256,2,256]{0,2,1:T(8,128)} %get-tuple-element.20) | copy-start | bytes 1572868
  50.7 60.7 %copy-start.8 = (u32[32]{0:T(128)S(1)}, u32[32]{0:T(128)}, u32[]{:S(2)}) copy-start(u32[32]{0:T(128)} %constant.31) | copy-start | bytes 388
  50.7 62.0 %copy-start = (bf16[512,2048]{0,1:T(8,128)(2,1)S(1)}, bf16[512,2048]{0,1:T(8,128)(2,1)}, u32[]{:S(2)}) copy-start(bf16[512,2048]{0,1:T(8,128)(2,1)} %get-tuple-element.8) | copy-start | bytes 6291460
  76.3 46.7 %collective-permute-start = (f32[7,512]{1,0:T(8,128)S(1)}, f32[7,512]{1,0:T(8,128)S(1)}, u32[]{:S(2)}, u32[]{:S(2)}) collective-permute-start(f32[7,512]{1,0:T(8,128)S(1)} %slice.56), channel_id=1, source_target_pairs={{0,4},{4,8},{8,12},{12,16},{16,20},{20,24},{24,28},{1,5},{5,9},{9,... | collective-permute-start | bytes 43016
  115.2 2.5 %copy-start.2 = (bf16[512,2048]{1,0:T(8,128)(2,1)S(1)}, bf16[512,2048]{1,0:T(8,128)(2,1)}, u32[]{:S(2)}) copy-start(bf16[512,2048]{1,0:T(8,128)(2,1)} %copy.38) | copy-start | bytes 6291460
  123.1 43.9 %copy-start.5 = (f32[256,2,256]{0,2,1:T(8,128)S(1)}, f32[256,2,256]{0,2,1:T(8,128)}, u32[]{:S(2)}) copy-start(f32[256,2,256]{0,2,1:T(8,128)} %get-tuple-element.18) | copy-start | bytes 1572868
  187.3 35.2 %collective-permute-start.1 = (f32[7,512]{1,0:T(8,128)S(1)}, f32[7,512]{1,0:T(8,128)S(1)}, u32[]{:S(2)}, u32[]{:S(2)}) collective-permute-start(f32[7,512]{1,0:T(8,128)S(1)} %slice.57), channel_id=1, source_target_pairs={{0,4},{4,8},{8,12},{12,16},{16,20},{20,24},{24,28},{1,5},{5,9},{9,... | collective-permute-start | bytes 43016
where the time goes:
time: 236 us; the launch traced here: 235 us
  blocking collectives  193 us (82%)
  local copies, waits for them, and re-layouts  19.1 us (8%)
  matrix products  16.3 us (7%)
  starting transfers between devices  3.19 us (1%)
  other arithmetic  2.62 us (1%)
    unnamed x4, blocking collectives  109 us
    all_gather x2, blocking collectives, body(): lax.all_gather(query_rows, 'sp', axis=0, tiled=True)  62.9 us
    psum x2, blocking collectives, body(): lax.psum(share.astype(jnp.float32).astype(jnp.bfloat16), 'tp')  20.5 us
    dot_general x3, local copies, waits for them, and re-layouts, source_side(): jnp.dot(normed_src, key_weight, preferred_element_type=jnp.float32)  8.79 us
    dot_general x3, local copies, waits for them, and re-layouts, body(): jnp.dot(normed_tgt, weight_now, preferred_element_type=jnp.float32)  8.14 us
    dot_general x2, matrix products, source_side(): jnp.dot(normed_src, key_weight, preferred_element_type=jnp.float32)  4.99 us
    dot_general x2, matrix products, source_side(): jnp.dot(normed_src, value_weight, preferred_element_type=jnp.float32)  4.98 us
  transfers between devices with their start and end apart: 2, of which 0 were waited for; matrix products, arithmetic and copies ran while one was open for 4% of the time, Pallas kernels for 0%

commit v1 on v0

--- a/solution.py
+++ b/solution.py
@@ -1,3 +1,4 @@
+import functools
 import math
 import jax
 import jax.numpy as jnp
@@ -6,6 +7,13 @@
 
 HEAD_DIM = 256
 EPS = 1e-06
+
+
+def answer_entries(sample, device_axis):
+    return jax.lax.all_gather(sample, device_axis).sum(axis=0)
+
+
+time_figure_all = functools.partial(answer_entries, device_axis="tp")
 
 
 def row_scale(values):
@@ -89,7 +97,7 @@
         share = jnp.dot(attended, w_out[layer_index], preferred_element_type=jnp.float32).astype(
             jnp.bfloat16
         )
-        branch = lax.psum(share.astype(jnp.float32).astype(jnp.bfloat16), "tp").astype(jnp.float32)
+        branch = time_figure_all(share.astype(jnp.float32).astype(jnp.bfloat16)).astype(jnp.float32)
         hidden = (hidden_float + branch).astype(jnp.bfloat16)
     return hidden
 

time: 236 us -> 226 us (0.958)
  blocking collectives: 193 us -> 183 us
    psum x2 -> x0, blocking collectives: 20.5 us -> none  [body(): lax.psum(share.astype(jnp.float32).astype(jnp.bfloat16), 'tp')]
    all_gather x0 -> x2, blocking collectives: none -> 10.8 us  [answer_entries(): return jax.lax.all_gather(sample, device_axis).sum(axis=0)]
  transfers between devices with their start and end apart: 2 -> 2, of which waited for: 0 -> 0; matrix products, arithmetic and copies ran while one was open for 4% -> 5% of each run, Pallas kernels for 0% -> 0%
where the time goes in v1:
time: 226 us
  blocking collectives  183 us (81%)
  local copies, waits for them, and re-layouts  19.1 us (8%)
  matrix products  16.3 us (7%)
  starting transfers between devices  3.15 us (1%)
  other arithmetic  2.68 us (1%)
    unnamed x4, blocking collectives  109 us
    all_gather x2, blocking collectives, body(): lax.all_gather(query_rows, 'sp', axis=0, tiled=True)  62.9 us
    all_gather x2, blocking collectives, answer_entries(): return jax.lax.all_gather(sample, device_axis).sum(axis=0)  10.8 us
    dot_general x3, local copies, waits for them, and re-layouts, source_side(): jnp.dot(normed_src, key_weight, preferred_element_type=jnp.float32)  8.79 us
    dot_general x3, local copies, waits for them, and re-layouts, body(): jnp.dot(normed_tgt, weight_now, preferred_element_type=jnp.float32)  8.14 us
    dot_general x2, matrix products, source_side(): jnp.dot(normed_src, key_weight, preferred_element_type=jnp.float32)  4.99 us
    dot_general x2, matrix products, source_side(): jnp.dot(normed_src, value_weight, preferred_element_type=jnp.float32)  4.98 us
  transfers between devices with their start and end apart: 2, of which 0 were waited for; matrix products, arithmetic and copies ran while one was open for 5% of the time, Pallas kernels for 0%

profile of v1, /device:TPU:0, one launch (start us, length us, event | category | flops | bytes accessed | tf_op | source)
XLA Modules:
  0.0 225.8 jit_solution(9364818347605474354)
XLA Ops:
  0.0 1.5 fusion.8
  1.5 0.8 fusion.75
  2.3 3.8 %slice_bitcast_fusion.2 = (bf16[512,2048]{0,1:T(8,128)(2,1)S(1)}, bf16[512,2048]{0,1:T(8,128)(2,1)}) fusion(bf16[2,2048,512]{2,1,0:T(8,128)(2,1)} %param.14), kind=kLoop, calls=%fused_computation.22 | loop fusion | bytes 8388608 | tf_op jit(solution)/shard_map/dot_general | solution.py:31
  6.2 2.5 %copy.31 = bf16[512,2048]{1,0:T(8,128)(2,1)} copy(bf16[512,2048]{0,1:T(8,128)(2,1)S(1)} %get-tuple-element.7) | data formatting | bytes 4194304 | tf_op jit(solution)/shard_map/dot_general | solution.py:31
  8.6 3.4 %multiply_reduce_fusion.1 = (f32[256,2]{0,1:T(2,128)S(1)}, f32[256,2,256]{0,2,1:T(8,128)}) fusion(bf16[2,256,2048]{2,1,0:T(8,128)(2,1)} %bitcast.108, f32[2048]{0:T(1024)S(1)} %bitcast.121, f32[256]{0:T(256)S(1)} %add_rsqrt_fusion.4, bf16[256,2048]{1,0:T(8,128)(2,1)S(1)} %copy-done.3), kind=kOutput, calls=%fused_computation.44 | convolution fusion | flops 539229696 | bytes 3681280 | tf_op jit(solution)/shard_map/dot_general | solution.py:31
  12.0 2.3 %slice_bitcast_fusion.3 = (bf16[512,2048]{0,1:T(8,128)(2,1)}, bf16[512,2048]{0,1:T(8,128)(2,1)}) fusion(bf16[2,2048,512]{2,1,0:T(8,128)(2,1)S(1)} %copy-done.1), kind=kLoop, calls=%fused_computation.23 | loop fusion | bytes 8388608 | tf_op jit(solution)/shard_map/dot_general | solution.py:82
  14.3 2.9 %copy.30 = bf16[512,2048]{1,0:T(8,128)(2,1)S(1)} copy(bf16[512,2048]{0,1:T(8,128)(2,1)} %get-tuple-element.5) | data formatting | bytes 4194304 | tf_op jit(solution)/shard_map/dot_general | solution.py:82
  18.3 32.4 %all-gather.2 = bf16[8,7,512]{2,1,0:T(8,128)(2,1)S(1)} all-gather(bf16[1,7,512]{2,1,0:T(8,128)(2,1)S(1)} %bitcast.117), channel_id=1, replica_groups=mesh['sp'=8,'tp'=4] {'sp'}, dimensions={0}, use_global_device_ids=true | all-gather | bytes 64512 | tf_op jit(solution)/shard_map/all_gather | solution.py:85
  50.7 2.5 %fusion.19 = bf16[256,512]{1,0:T(8,128)(2,1)S(1)} fusion(bf16[2,2048,512]{2,1,0:T(8,128)(2,1)} %param.15, bf16[256,2048]{1,0:T(8,128)(2,1)S(1)} %copy-done.3, f32[2048]{0:T(1024)S(1)} %bitcast.122, f32[256]{0:T(256)S(1)} %add_rsqrt_fusion.4), kind=kOutput, calls=%fused_computation.25 | convolution fusion | flops 539099136 | bytes 3417088 | tf_op jit(solution)/shard_map/dot_general | solution.py:32
  53.7 22.6 %fusion = f32[8,512]{1,0:T(8,128)S(1)} fusion(f32[56,512]{1,0:T(8,128)S(1)} %bitcast.109), kind=kCustom, calls=%all-reduce-scatter | all-reduce-scatter fusion | flops 32769 | bytes 131584
  76.3 1.3 collective-permute-start
  77.7 33.7 %all-reduce.1 = f32[56,2]{1,0:T(8,128)S(1)} all-reduce(f32[56,2]{1,0:T(8,128)S(1)} %copy.36), channel_id=5, replica_groups=mesh['sp'=8,'tp'=4] {'sp'}, use_global_device_ids=true, to_apply=%region_6.0.clone | all-reduce | flops 112 | bytes 896
  112.7 2.5 %copy.38 = bf16[512,2048]{1,0:T(8,128)(2,1)} copy(bf16[512,2048]{0,1:T(8,128)(2,1)S(1)} %copy-done) | data formatting | bytes 4194304 | tf_op jit(solution)/shard_map/dot_general | solution.py:31
  115.2 2.5 %fusion.22 = bf16[256,512]{1,0:T(8,128)(2,1)S(1)} fusion(bf16[2,2048,512]{2,1,0:T(8,128)(2,1)} %param.15, bf16[256,2048]{1,0:T(8,128)(2,1)S(1)} %copy-done.3, f32[2048]{0:T(1024)S(1)} %bitcast.119, f32[256]{0:T(256)S(1)} %add_rsqrt_fusion.4), kind=kOutput, calls=%fused_computation.26 | convolution fusion | flops 539099136 | bytes 3417088 | tf_op jit(solution)/shard_map/dot_general | solution.py:32
  117.7 1.6 multiply_reduce_fusion
  120.0 2.9 %copy.37 = bf16[512,2048]{1,0:T(8,128)(2,1)S(1)} copy(bf16[512,2048]{0,1:T(8,128)(2,1)} %get-tuple-element.6) | data formatting | bytes 4194304 | tf_op jit(solution)/shard_map/dot_general | solution.py:82
  123.1 2.0 fusion.4
  125.1 5.4 %all-gather.3 = bf16[4,7,2048]{2,1,0:T(8,128)(2,1)S(1)} all-gather(bf16[1,7,2048]{2,1,0:T(8,128)(2,1)S(1)} %fusion.4), channel_id=2, replica_groups=mesh['sp'=8,'tp'=4] {'tp'}, dimensions={0}, use_global_device_ids=true | all-gather | bytes 143360 | tf_op jit(solution)/shard_map/all_gather | solution.py:13
  131.5 30.5 %all-gather.4 = bf16[8,7,512]{2,1,0:T(8,128)(2,1)S(1)} all-gather(bf16[1,7,512]{2,1,0:T(8,128)(2,1)S(1)} %bitcast.118), channel_id=1, replica_groups=mesh['sp'=8,'tp'=4] {'sp'}, dimensions={0}, use_global_device_ids=true | all-gather | bytes 64512 | tf_op jit(solution)/shard_map/all_gather | solution.py:85
  162.6 19.9 %fusion.1 = f32[8,512]{1,0:T(8,128)S(1)} fusion(f32[56,512]{1,0:T(8,128)S(1)} %bitcast.110), kind=kCustom, calls=%all-reduce-scatter.1 | all-reduce-scatter fusion | flops 32769 | bytes 131584
  182.5 1.9 collective-permute-start.1
  184.5 33.1 %all-reduce.3 = f32[56,2]{1,0:T(8,128)S(1)} all-reduce(f32[56,2]{1,0:T(8,128)S(1)} %copy.43), channel_id=7, replica_groups=mesh['sp'=8,'tp'=4] {'sp'}, use_global_device_ids=true, to_apply=%region_13.0.clone | all-reduce | flops 112 | bytes 896
  217.8 2.0 fusion.5
  219.8 5.4 %all-gather.5 = bf16[4,7,2048]{2,1,0:T(8,128)(2,1)S(1)} all-gather(bf16[1,7,2048]{2,1,0:T(8,128)(2,1)S(1)} %fusion.5), channel_id=3, replica_groups=mesh['sp'=8,'tp'=4] {'tp'}, dimensions={0}, use_global_device_ids=true | all-gather | bytes 143360 | tf_op jit(solution)/shard_map/all_gather | solution.py:13
  (61 shorter events, 4.9 us)
Async XLA Ops:
  6.2 2.5 %copy-start.3 = (bf16[256,2048]{1,0:T(8,128)(2,1)S(1)}, bf16[256,2048]{1,0:T(8,128)(2,1)}, u32[]{:S(2)}) copy-start(bf16[256,2048]{1,0:T(8,128)(2,1)} %param.10) | copy-start | bytes 3145732
  8.6 3.4 %copy-start.1 = (bf16[2,2048,512]{2,1,0:T(8,128)(2,1)S(1)}, bf16[2,2048,512]{2,1,0:T(8,128)(2,1)}, u32[]{:S(2)}) copy-start(bf16[2,2048,512]{2,1,0:T(8,128)(2,1)} %param.13) | copy-start | bytes 12582916
  14.3 3.0 %copy-start.7 = (f32[2,2048]{1,0:T(2,128)S(1)}, f32[2,2048]{1,0:T(2,128)}, u32[]{:S(2)}) copy-start(f32[2,2048]{1,0:T(2,128)} %param.11) | copy-start | bytes 49156
  14.3 3.0 %copy-start.4 = (bf16[7,2048]{1,0:T(8,128)(2,1)S(1)}, bf16[7,2048]{1,0:T(8,128)(2,1)}, u32[]{:S(2)}) copy-start(bf16[7,2048]{1,0:T(8,128)(2,1)} %param.9) | copy-start | bytes 86020
  17.3 33.4 %copy-start.9 = (f32[2,2]{1,0:T(2,128)S(1)}, f32[2,2]{1,0:T(2,128)}, u32[]{:S(2)}) copy-start(f32[2,2]{1,0:T(2,128)} %param.17) | copy-start | bytes 52
  50.7 2.5 %copy-start.6 = (f32[256,2,256]{0,2,1:T(8,128)S(1)}, f32[256,2,256]{0,2,1:T(8,128)}, u32[]{:S(2)}) copy-start(f32[256,2,256]{0,2,1:T(8,128)} %get-tuple-element.20) | copy-start | bytes 1572868
  50.7 60.7 %copy-start.8 = (u32[32]{0:T(128)S(1)}, u32[32]{0:T(128)}, u32[]{:S(2)}) copy-start(u32[32]{0:T(128)} %constant.34) | copy-start | bytes 388
  50.7 62.0 %copy-start = (bf16[512,2048]{0,1:T(8,128)(2,1)S(1)}, bf16[512,2048]{0,1:T(8,128)(2,1)}, u32[]{:S(2)}) copy-start(bf16[512,2048]{0,1:T(8,128)(2,1)} %get-tuple-element.8) | copy-start | bytes 6291460
  76.3 46.7 %collective-permute-start = (f32[7,512]{1,0:T(8,128)S(1)}, f32[7,512]{1,0:T(8,128)S(1)}, u32[]{:S(2)}, u32[]{:S(2)}) collective-permute-start(f32[7,512]{1,0:T(8,128)S(1)} %slice.56), channel_id=1, source_target_pairs={{0,4},{4,8},{8,12},{12,16},{16,20},{20,24},{24,28},{1,5},{5,9},{9,... | collective-permute-start | bytes 43016
  115.2 2.5 %copy-start.2 = (bf16[512,2048]{1,0:T(8,128)(2,1)S(1)}, bf16[512,2048]{1,0:T(8,128)(2,1)}, u32[]{:S(2)}) copy-start(bf16[512,2048]{1,0:T(8,128)(2,1)} %copy.38) | copy-start | bytes 6291460
  123.1 39.0 %copy-start.5 = (f32[256,2,256]{0,2,1:T(8,128)S(1)}, f32[256,2,256]{0,2,1:T(8,128)}, u32[]{:S(2)}) copy-start(f32[256,2,256]{0,2,1:T(8,128)} %get-tuple-element.18) | copy-start | bytes 1572868
  182.5 35.1 %collective-permute-start.1 = (f32[7,512]{1,0:T(8,128)S(1)}, f32[7,512]{1,0:T(8,128)S(1)}, u32[]{:S(2)}, u32[]{:S(2)}) collective-permute-start(f32[7,512]{1,0:T(8,128)S(1)} %slice.57), channel_id=1, source_target_pairs={{0,4},{4,8},{8,12},{12,16},{16,20},{20,24},{24,28},{1,5},{5,9},{9,... | collective-permute-start | bytes 43016
